TPU v7x, 32 devices: a whole 2x2x4 slice. The times are simulated.
32 devices in a mesh: fs: 8 (over z, y), tp: 4 (over x, core).
Axes of the slice: x: 2, y: 2, z: 4, core: 2. Of those that a mesh axis runs over, the one named last changes fastest.
Arguments:
- resid: bfloat16 [8192, 2048], P(('fs', 'tp')), may hold values from -6 to 6
- mix_gain: float32 [2048], replicated, may hold values from 0.1 to 1.9
- w_query: bfloat16 [2048, 1024], P('fs', 'tp'), may hold values from -0.125 to 0.125
- w_key: bfloat16 [2048, 1024], P('fs', 'tp'), may hold values from -0.125 to 0.125
- w_value: bfloat16 [2048, 2048], P('fs', 'tp'), may hold values from -0.125 to 0.125
- w_gate: bfloat16 [2048, 2048], P('fs', 'tp'), may hold values from -0.125 to 0.125
- w_output: bfloat16 [2048, 2048], P('tp', 'fs'), may hold values from -0.125 to 0.125
- decay_rate: float32 [8], P('tp'), may hold values from 0.0008 to 0.034, as said below
- mlp_gain: float32 [2048], replicated, may hold values from 0.1 to 1.9
- w_up: bfloat16 [2048, 8192], P('fs', 'tp'), may hold values from -0.125 to 0.125
- w_down: bfloat16 [8192, 2048], P('tp', 'fs'), may hold values from -0.0625 to 0.0625
Outputs:
- layer_out: bfloat16 [8192, 2048], P(('fs', 'tp'))
Inputs may be any that keep to these rules, and one draw needn't show every extreme that they name: `decay_rate`: decay rates per position, one for each head.
All inputs are finite; a program needn't handle non-finite values.
Results may differ from a plain program's by a relative error of at most 0.038.
Values may be sent and summed in bfloat16 or wider, within the bound.
A program may use at most 64 MiB of HBM per device.

v0:
```python
import jax
import jax.numpy as jnp
from jax import lax
from jax.sharding import PartitionSpec as P

DK = 128
DV = 256
BLOCK = 128
LENGTH = 512


epsilon = 1e-06


def rms_scale(source, gains):
    widened = source.astype(jnp.float32)
    scaled = widened * lax.rsqrt(jnp.mean(widened * widened, axis=-1, keepdims=True) + epsilon)
    return (scaled * gains).astype(jnp.bfloat16)


def retention(queries, key_rows, values, rates):
    seq_count, length, head_count, key_width = queries.shape
    value_width = values.shape[-1]
    block_count = length // BLOCK
    queries = queries.reshape(seq_count, block_count, BLOCK, head_count, key_width)
    key_rows = key_rows.reshape(
        seq_count, block_count, BLOCK, head_count, key_width
    ) * key_width ** (-0.5)
    values = values.reshape(seq_count, block_count, BLOCK, head_count, value_width)
    places = jnp.arange(BLOCK, dtype=jnp.float32)
    offset = places[:, None] - places[None, :]
    causal = offset >= 0
    inner_decay = jnp.where(
        causal[None], jnp.exp(-rates[:, None, None] * jnp.where(causal, offset, 0.0)[None]), 0.0
    )
    scores = jnp.einsum("bnihd,bnjhd->bnhij", queries, key_rows) * inner_decay[None, None]
    within = jnp.einsum("bnhij,bnjhe->bnihe", scores, values)
    key_decayed = (
        key_rows
        * jnp.exp(-rates[None, :] * (BLOCK - 1.0 - places)[:, None])[None, None, :, :, None]
    )
    updates = jnp.einsum("bnjhd,bnjhe->nbhde", key_decayed, values)
    carry_decay = jnp.exp(-rates * BLOCK)[None, :, None, None]

    def advance(memory, update):
        return (carry_decay * memory + update, memory)

    _, before = lax.scan(
        advance, jnp.zeros((seq_count, head_count, key_width, value_width), jnp.float32), updates
    )
    query_decayed = (
        queries * jnp.exp(-rates[None, :] * (places + 1.0)[:, None])[None, None, :, :, None]
    )
    carried = jnp.einsum("bnihd,nbhde->bnihe", query_decayed, before)
    mixed = (within + carried).reshape(seq_count, length, head_count, value_width)
    centre = jnp.mean(mixed, axis=-1, keepdims=True)
    spread = jnp.mean(jnp.square(mixed - centre), axis=-1, keepdims=True)
    return (mixed - centre) * lax.rsqrt(spread + epsilon)


def heads_view(source, width):
    return source.astype(jnp.float32).reshape(-1, LENGTH, source.shape[1] // width, width)


def on_device(
    resid, mix_gain, w_query, w_key, w_value, w_gate, w_output, decay_rate, mlp_gain, w_up, w_down
):
    normed = lax.all_gather(rms_scale(resid, mix_gain), "tp", axis=0, tiled=True)
    tokens = normed.shape[0]
    pieces = (
        lax.all_gather(w_query, "fs", axis=0, tiled=True),
        lax.all_gather(w_key, "fs", axis=0, tiled=True),
        lax.all_gather(w_value, "fs", axis=0, tiled=True),
        lax.all_gather(w_gate, "fs", axis=0, tiled=True),
    )
    columns = normed
    projected = tuple(
        (jnp.dot(columns, shard_rows, preferred_element_type=jnp.float32) for shard_rows in pieces)
    )
    queries, key_rows, values, gate_rows = (
        member_sum.astype(jnp.bfloat16) for member_sum in projected
    )
    output_whole = lax.all_gather(w_output, "fs", axis=1, tiled=True)
    grouped = retention(
        heads_view(queries, DK), heads_view(key_rows, DK), heads_view(values, DV), decay_rate
    )
    gated = (jax.nn.silu(gate_rows.astype(jnp.float32)) * grouped.reshape(tokens, -1)).astype(
        jnp.bfloat16
    )
    mix_sum = lax.psum_scatter(
        jnp.dot(gated, output_whole, preferred_element_type=jnp.float32).astype(jnp.bfloat16),
        "tp",
        scatter_dimension=0,
        tiled=True,
    ).astype(jnp.float32)
    after_mix = (resid.astype(jnp.float32) + mix_sum).astype(jnp.bfloat16)
    normed_mlp = lax.all_gather(rms_scale(after_mix, mlp_gain), "tp", axis=0, tiled=True)
    columns = normed_mlp
    lifted = jnp.dot(
        columns, lax.all_gather(w_up, "fs", axis=0, tiled=True), preferred_element_type=jnp.float32
    )
    down_whole = lax.all_gather(w_down, "fs", axis=1, tiled=True)
    hidden = jnp.square(jax.nn.relu(lifted)).astype(jnp.bfloat16)
    mlp_sum = lax.psum_scatter(
        jnp.dot(hidden, down_whole, preferred_element_type=jnp.float32).astype(jnp.bfloat16),
        "tp",
        scatter_dimension=0,
        tiled=True,
    ).astype(jnp.float32)
    return (after_mix.astype(jnp.float32) + mlp_sum).astype(jnp.bfloat16)


def solution(mesh):
    placed = (
        P(("fs", "tp"), None),
        P(),
        P("fs", "tp"),
        P("fs", "tp"),
        P("fs", "tp"),
        P("fs", "tp"),
        P("tp", "fs"),
        P("tp"),
        P(),
        P("fs", "tp"),
        P("tp", "fs"),
    )
    return jax.shard_map(
        on_device, mesh=mesh, in_specs=placed, out_specs=P(("fs", "tp"), None), check_vma=False
    )
```

profile of v0, /device:TPU:0, one launch (start us, length us, event | category | flops | bytes accessed | tf_op | source)
XLA Modules:
  0.0 699.5 jit_solution(10212446089821985571)
XLA Ops:
  7.3 1.5 fusion.4
  8.8 2.5 fusion.6
  14.2 38.3 %all-gather.18.cloned.1.call-done = bf16[2048,256]{1,0:T(8,128)(2,1)} async-done(((bf16[256,256]{1,0:T(8,128)(2,1)}), bf16[2048,256]{1,0:T(8,128)(2,1)}) %all-gather.18.cloned.1.call-update) | async-done | bytes 1048592 | tf_op jit(solution)/shard_map/all_gather | solution.py:72
  52.5 34.8 %all-gather.10.cloned.1.call-done = bf16[1024,2048]{1,0:T(8,128)(2,1)} async-done(((bf16[256,2048]{1,0:T(8,128)(2,1)}), bf16[1024,2048]{1,0:T(8,128)(2,1)}) %all-gather.10.cloned.1.call-update) | async-done | bytes 4194320 | tf_op jit(solution)/shard_map/all_gather | solution.py:68
  87.2 3.7 fusion.13
  91.6 1.5 copy.28
  93.0 45.5 %all-gather.14.cloned.1.call-done = bf16[2048,512]{1,0:T(8,128)(2,1)} async-done(((bf16[256,512]{1,0:T(8,128)(2,1)}), bf16[2048,512]{1,0:T(8,128)(2,1)}) %all-gather.14.cloned.1.call-update) | async-done | bytes 2097168 | tf_op jit(solution)/shard_map/all_gather | solution.py:73
  138.5 5.2 convolution_convert_fusion.2
  143.7 1.1 reshape_reshape.15
  144.9 34.5 %all-gather.16.cloned.1.call-done = bf16[2048,256]{1,0:T(8,128)(2,1)} async-done(((bf16[256,256]{1,0:T(8,128)(2,1)}), bf16[2048,256]{1,0:T(8,128)(2,1)}) %all-gather.16.cloned.1.call-update) | async-done | bytes 1048592 | tf_op jit(solution)/shard_map/all_gather | solution.py:71
  179.3 3.7 convolution_convert_fusion.5
  184.0 2.0 fusion.14
  186.0 3.6 while.13
  189.6 3.4 fusion.17
  193.0 2.9 fusion.37
  195.9 2.4 copy.32
  198.8 1.2 mul.177
  200.4 1.2 sub.61
  201.7 1.6 copy.44
  204.0 1.5 copy.43
  205.5 23.6 %all-gather.12.cloned.1.call-done = bf16[2048,512]{1,0:T(8,128)(2,1)} async-done(((bf16[256,512]{1,0:T(8,128)(2,1)}), bf16[2048,512]{1,0:T(8,128)(2,1)}) %all-gather.12.cloned.1.call-update) | async-done | bytes 2097168 | tf_op jit(solution)/shard_map/all_gather | solution.py:74
  229.1 50.8 %all-gather.20.cloned.1.call-done = bf16[512,2048]{1,0:T(8,128)(2,1)} async-done(((bf16[512,256]{1,0:T(8,128)(2,1)}), bf16[512,2048]{1,0:T(8,128)(2,1)}) %all-gather.20.cloned.1.call-update) | async-done | bytes 2097168 | tf_op jit(solution)/shard_map/all_gather | solution.py:83
  279.9 11.3 %convolution_convert_fusion.1 = bf16[1024,2048]{1,0:T(8,128)(2,1)} fusion(bf16[512,2048]{1,0:T(8,128)(2,1)} %all-gather.20.cloned.1.call-done, f32[1024,512]{1,0:T(8,128)S(1)} %bitcast.46, f32[1024,512]{1,0:T(8,128)} %bitcast.48, f32[1024,512]{1,0:T(8,128)} %bitcast.47, bf16[1024,2048]{1,0:T(8,128)(2,1)} %all-gather.10.cloned.1.call-done, ...), kind=kOutput, calls=%fused_computation.4 | convolution fusion | flops 4302307328 | bytes 18874368 | tf_op jit(solution)/shard_map/dot_general | solution.py:91
  292.8 41.3 %reduce-scatter.3.cloned.1.call-done = bf16[256,2048]{1,0:T(8,128)(2,1)} async-done(((bf16[1024,2048]{1,0:T(8,128)(2,1)}), bf16[256,2048]{1,0:T(8,128)(2,1)}) %reduce-scatter.3.cloned.1.call-update) | async-done | bytes 1048592 | tf_op jit(solution)/shard_map/reduce_scatter | solution.py:90
  334.2 1.7 fusion.8
  336.0 1.5 fusion.10
  337.5 123.3 %all-gather.24.cloned.1.call-done = bf16[2048,2048]{1,0:T(8,128)(2,1)} async-done(((bf16[256,2048]{1,0:T(8,128)(2,1)}), bf16[2048,2048]{1,0:T(8,128)(2,1)}) %all-gather.24.cloned.1.call-update) | async-done | bytes 8388624 | tf_op jit(solution)/shard_map/all_gather | solution.py:100
  460.8 125.2 %all-gather.26.cloned.1.call-done = bf16[2048,2048]{1,0:T(8,128)(2,1)} async-done(((bf16[2048,256]{1,0:T(8,128)(2,1)}), bf16[2048,2048]{1,0:T(8,128)(2,1)}) %all-gather.26.cloned.1.call-update) | async-done | bytes 8388624 | tf_op jit(solution)/shard_map/all_gather | solution.py:102
  586.0 34.1 %all-gather.22.cloned.1.call-done = bf16[1024,2048]{1,0:T(8,128)(2,1)} async-done(((bf16[256,2048]{1,0:T(8,128)(2,1)}), bf16[1024,2048]{1,0:T(8,128)(2,1)}) %all-gather.22.cloned.1.call-update) | async-done | bytes 4194320 | tf_op jit(solution)/shard_map/all_gather | solution.py:97
  620.1 25.4 %convolution_convert_fusion = bf16[1024,2048]{1,0:T(8,128)(2,1)} fusion(bf16[2048,2048]{1,0:T(8,128)(2,1)} %all-gather.26.cloned.1.call-done, bf16[1024,2048]{1,0:T(8,128)(2,1)} %all-gather.22.cloned.1.call-done, bf16[2048,2048]{1,0:T(8,128)(2,1)} %all-gather.24.cloned.1.call-done), kind=kOutput, calls=%fused_computation.3 | convolution fusion | flops 17188257792 | bytes 25165824 | tf_op jit(solution)/shard_map/dot_general | solution.py:105
  645.5 44.8 %reduce-scatter.5.cloned.1.call-done = bf16[256,2048]{1,0:T(8,128)(2,1)} async-done(((bf16[1024,2048]{1,0:T(8,128)(2,1)}), bf16[256,2048]{1,0:T(8,128)(2,1)}) %reduce-scatter.5.cloned.1.call-update) | async-done | bytes 1048592 | tf_op jit(solution)/shard_map/reduce_scatter | solution.py:104
  690.3 2.7 fusion.11
  (62 shorter events, 11.7 us)
Async XLA Ops:
  6.5 46.0 %all-gather.18.cloned.1.call-start = ((), (), s32[]{:S(2)}) async-start(), calls=%async_computation.6 | async-start | bytes 1179648 | tf_op jit(solution)/shard_map/all_gather | solution.py:72
  7.3 80.0 %all-gather.10.cloned.1.call-start = ((), (), s32[]{:S(2)}) async-start(), calls=%async_computation.2 | async-start | bytes 5242880 | tf_op jit(solution)/shard_map/all_gather | solution.py:68
  8.8 5.2 copy-start.6
  11.4 127.1 %all-gather.14.cloned.1.call-start = ((), (), s32[]{:S(2)}) async-start(), calls=%async_computation.4 | async-start | bytes 2359296 | tf_op jit(solution)/shard_map/all_gather | solution.py:73
  12.1 167.2 %all-gather.16.cloned.1.call-start = ((), (), s32[]{:S(2)}) async-start(), calls=%async_computation.5 | async-start | bytes 1179648 | tf_op jit(solution)/shard_map/all_gather | solution.py:71
  12.7 216.4 %all-gather.12.cloned.1.call-start = ((), (), s32[]{:S(2)}) async-start(), calls=%async_computation.3 | async-start | bytes 2359296 | tf_op jit(solution)/shard_map/all_gather | solution.py:74
  13.3 266.6 %all-gather.20.cloned.1.call-start = ((), (), s32[]{:S(2)}) async-start(), calls=%async_computation.7 | async-start | bytes 2359296 | tf_op jit(solution)/shard_map/all_gather | solution.py:83
  13.9 320.3 %reduce-scatter.3.cloned.1.call-start = ((), (), s32[]{:S(2)}) async-start(), calls=%async_computation.8 | async-start | bytes 5242880 | tf_op jit(solution)/shard_map/reduce_scatter | solution.py:90
  91.5 52.2 %copy-start.2 = (f32[2,4,128,2,128]{4,3,2,1,0:T(2,128)}, f32[2,4,128,2,128]{4,3,2,1,0:T(2,128)S(1)}, u32[]{:S(2)}) copy-start(f32[2,4,128,2,128]{4,3,2,1,0:T(2,128)S(1)} %reshape.152) | copy-start | bytes 3145732
  189.6 3.4 copy-start.1
  201.7 2.3 copy-start.4
  291.3 42.9 %copy-start = (bf16[256,2048]{1,0:T(8,128)(2,1)S(1)}, bf16[256,2048]{1,0:T(8,128)(2,1)}, u32[]{:S(2)}) copy-start(bf16[256,2048]{1,0:T(8,128)(2,1)} %param.13) | copy-start | bytes 3145732
  291.3 44.6 %copy-start.5 = (f32[2048]{0:T(1024)S(1)}, f32[2048]{0:T(1024)}, u32[]{:S(2)}) copy-start(f32[2048]{0:T(1024)} %param.21) | copy-start | bytes 24580
  291.3 169.5 %all-gather.24.cloned.1.call-start = ((), (), s32[]{:S(2)}) async-start(), calls=%async_computation.10 | async-start | bytes 9437184 | tf_op jit(solution)/shard_map/all_gather | solution.py:100
  292.1 294.0 %all-gather.26.cloned.1.call-start = ((), (), s32[]{:S(2)}) async-start(), calls=%async_computation.11 | async-start | bytes 9437184 | tf_op jit(solution)/shard_map/all_gather | solution.py:102
  292.8 327.3 %all-gather.22.cloned.1.call-start = ((), (), s32[]{:S(2)}) async-start(), calls=%async_computation.9 | async-start | bytes 5242880 | tf_op jit(solution)/shard_map/all_gather | solution.py:97
  334.2 1.8 copy-start.3
  337.5 352.8 %reduce-scatter.5.cloned.1.call-start = ((), (), s32[]{:S(2)}) async-start(), calls=%async_computation.12 | async-start | bytes 5242880 | tf_op jit(solution)/shard_map/reduce_scatter | solution.py:104
Sparse Core Ops, SparseCore 0:
  9.5 42.9 all-gather.17
  54.0 33.1 all-gather.9
  89.4 49.0 all-gather.13
  140.5 38.7 all-gather.15
  181.3 47.7 all-gather.11
  231.0 48.8 all-gather.19
  291.4 42.7 reduce-scatter.2
  336.3 124.4 all-gather.23
  462.9 123.1 all-gather.25
  587.4 32.6 all-gather.21
  645.6 44.5 reduce-scatter.4
where the time goes:
time: 700 us
  waiting for transfers between devices  600 us (86%)
  matrix products  57.6 us (8%)
  other arithmetic  14 us (2%)
  local copies, waits for them, and re-layouts  13.5 us (2%)
  between operations  13.5 us (2%)
    all_gather x1, waiting for transfers between devices, on_device(): down_whole = lax.all_gather(w_down, 'fs', axis=1, tiled=True)  125 us
    all_gather x1, waiting for transfers between devices, on_device(): lax.all_gather(w_up, 'fs', axis=0, tiled=True)  123 us
    all_gather x1, waiting for transfers between devices, on_device(): output_whole = lax.all_gather(w_output, 'fs', axis=1, tiled=True)  50.8 us
    all_gather x1, waiting for transfers between devices, on_device(): lax.all_gather(w_value, 'fs', axis=0, tiled=True)  45.5 us
    reduce_scatter x1, waiting for transfers between devices, on_device(): lax.psum_scatter(jnp.dot(hidden, down_whole, preferred_element_type=jnp.f...  44.8 us
    reduce_scatter x1, waiting for transfers between devices, on_device(): lax.psum_scatter(jnp.dot(gated, output_whole, preferred_element_type=jnp....  41.3 us
    all_gather x1, waiting for transfers between devices, on_device(): lax.all_gather(w_key, 'fs', axis=0, tiled=True)  38.3 us
    all_gather x1, waiting for transfers between devices, on_device(): lax.all_gather(rms_scale(resid, mix_gain), 'tp', axis=0, tiled=True)  34.8 us
  transfers between devices with their start and end apart: 11, of which 11 were waited for; matrix products, arithmetic and copies ran while one was open for 6% of the time, Pallas kernels for 0%

commit v1 on v0

v1 whole, which is shorter than its diff:
```python
import functools

import jax
import jax.numpy as jnp
from jax import lax
from jax.experimental import pallas as pl
from jax.experimental.pallas import tpu as pltpu
from jax.sharding import PartitionSpec as P

DK = 128
DV = 256
LENGTH = 512
MESH = pl.DeviceIdType.MESH
EPS = 1e-06
F32 = jnp.float32
BF16 = jnp.bfloat16


def tile_of(width):
    return 256 if width % 256 == 0 else 128


def kernel(fs, tp, resid_ref, mix_gain_ref, mlp_gain_ref, rate_ref, wq_ref, wo_ref, wu_ref, wd_ref,
           out_ref, wq, wo, wu, wd, xn, xn2, proj, gated, hidden, part1, recv1, part2, recv2,
           after, ring_send, ring_recv, own_sem, ag_send, ag_recv, rs1_send, rs1_recv,
           rs2_send, rs2_recv):
    half = fs // 2
    rows = resid_ref.shape[0]
    heads = rate_ref.shape[0]
    tokens = rows * tp
    me_f = lax.axis_index("fs")
    me_t = lax.axis_index("tp")

    def place(i):
        col = i % 2
        line = i // 2
        return line * (1 - col) + (fs - 1 - line) * col

    def index(p):
        col = p // half
        return 2 * (p * (1 - col) + (fs - 1 - p) * col) + col

    my_place = place(me_f)
    target = (index((my_place + 1) % fs), index((my_place + fs - 1) % fs))

    def owner(way, dist):
        if way == 0:
            return index((my_place + fs - dist) % fs)
        return index((my_place + dist) % fs)

    def peer(d):
        return (me_t + d) % tp

    barrier = pltpu.get_barrier_semaphore()
    for way in range(2):
        pl.semaphore_signal(barrier, inc=1, device_id=(target[way], me_t), device_id_type=MESH)
    for d in range(1, tp):
        pl.semaphore_signal(barrier, inc=1, device_id=(me_f, peer(d)), device_id_type=MESH)
    pl.semaphore_wait(barrier, 2 + tp - 1)

    groups = ((wq_ref, wq, False), (wo_ref, wo, True), (wu_ref, wu, False), (wd_ref, wd, True))

    def slot(w, who, h):
        source, whole, slotted = groups[w]
        deep = source.shape[0]
        hr = deep // 2
        if slotted:
            return whole.at[who, pl.ds(h * hr, hr), :]
        return whole.at[pl.ds(pl.multiple_of(who * deep + h * hr, hr), hr), :]

    rounds = []
    for w in range(4):
        for dist in range(1, half):
            rounds += [(w, dist, 0), (w, dist, 1)]
        rounds.append((w, half, 0))
    per = fs - 1
    started = []

    def half_of(way, turn):
        return turn if way == 0 else 1 - turn

    def send(k):
        w, dist, turn = rounds[k]
        for way in range(2):
            h = half_of(way, turn)
            who = owner(way, dist - 1)
            source = groups[w][0]
            hr = source.shape[0] // 2
            src = source.at[pl.ds(h * hr, hr), :] if dist == 1 else slot(w, who, h)
            copy = pltpu.make_async_remote_copy(
                src_ref=src, dst_ref=slot(w, who, h), send_sem=ring_send.at[way, k],
                recv_sem=ring_recv.at[way, k], device_id=(target[way], me_t), device_id_type=MESH)
            copy.start()
            started.append(copy)

    def arrive(k):
        w, dist, turn = rounds[k]
        for way in range(2):
            h = half_of(way, turn)
            here = slot(w, owner(way, dist), h)
            pltpu.make_async_remote_copy(
                src_ref=here, dst_ref=here, send_sem=ring_send.at[way, k],
                recv_sem=ring_recv.at[way, k], device_id=(target[way], me_t),
                device_id_type=MESH).wait_recv()
        if dist + 1 < half or (dist + 1 == half and turn == 0):
            send(k + 2)

    own_at = {}
    own_at.setdefault(per - 3, []).append(per)
    own_at.setdefault(per - 2, []).append(per + 1)
    own_at.setdefault(per - 1, []).append(2 * per)
    own_at.setdefault(per + 3, []).append(2 * per + 1)
    own_at.setdefault(3 * per - 3, []).append(3 * per)
    own_at.setdefault(3 * per - 2, []).append(3 * per + 1)

    send(0)
    send(1)
    own = []
    for w in range(4):
        source, whole, slotted = groups[w]
        deep = source.shape[0]
        dst = whole.at[me_f] if slotted else whole.at[pl.ds(pl.multiple_of(me_f * deep, deep), deep), :]
        copy = pltpu.make_async_copy(source, dst, own_sem.at[w])
        copy.start()
        own.append(copy)

    my_rows = pl.ds(pl.multiple_of(me_t * rows, rows), rows)

    def norm(source, gain_ref):
        wide = source.astype(F32)
        mean = jnp.mean(wide * wide, axis=-1, keepdims=True)
        return (wide * lax.rsqrt(mean + EPS) * gain_ref[...]).astype(BF16)

    def ag_copy(which, buf, d, receiving):
        block = peer(tp - d) if receiving else me_t
        place_ = buf.at[pl.ds(pl.multiple_of(block * rows, rows), rows), :]
        return pltpu.make_async_remote_copy(
            src_ref=place_, dst_ref=place_, send_sem=ag_send.at[which, d - 1],
            recv_sem=ag_recv.at[which, d - 1], device_id=(me_f, peer(d)), device_id_type=MESH)

    def ag_start(which, buf):
        for d in range(1, tp):
            copy = ag_copy(which, buf, d, False)
            copy.start()
            started.append(copy)

    def ag_wait(which, buf):
        for d in range(1, tp):
            ag_copy(which, buf, d, True).wait_recv()

    step = 64

    def norm_into(buf, source_ref, gain_ref):
        @pl.loop(0, rows // step)
        def _(i):
            at = pl.multiple_of(i * step, step)
            buf[pl.ds(pl.multiple_of(me_t * rows + at, step), step), :] = norm(
                source_ref[pl.ds(at, step), :], gain_ref)

    def project():
        width = proj.shape[1]
        t = tile_of(width)

        @pl.loop(0, width // t)
        def _(j):
            cols = pl.ds(pl.multiple_of(j * t, t), t)
            proj[:, cols] = jnp.dot(xn[...], wq[:, cols], preferred_element_type=F32).astype(BF16)

    def retain():
        kq = heads * DK
        vq = heads * DV
        count = tokens // LENGTH
        for head in range(heads):
            rate = rate_ref[head:head + 1, 0:1]

            @pl.loop(0, count)
            def _(n):
                base = pl.multiple_of(n * LENGTH, LENGTH)
                rs = pl.ds(base, LENGTH)
                q = proj[rs, head * DK:(head + 1) * DK]
                k = proj[rs, kq + head * DK:kq + (head + 1) * DK]
                v = proj[rs, 2 * kq + head * DV:2 * kq + (head + 1) * DV]
                g = proj[rs, 2 * kq + vq + head * DV:2 * kq + vq + (head + 1) * DV].astype(F32)
                scores = lax.dot_general(q, k, (((1,), (1,)), ((), ())), preferred_element_type=F32)
                t_at = lax.broadcasted_iota(jnp.int32, (LENGTH, LENGTH), 0)
                s_at = lax.broadcasted_iota(jnp.int32, (LENGTH, LENGTH), 1)
                gap = t_at - s_at
                decay = jnp.exp(-rate * jnp.maximum(gap, 0).astype(F32)) * (DK ** -0.5)
                scores = jnp.where(gap >= 0, scores * decay, 0.0).astype(BF16)
                mixed = jnp.dot(scores, v, preferred_element_type=F32)
                mean = jnp.mean(mixed, axis=-1, keepdims=True)
                off = mixed - mean
                var = jnp.mean(off * off, axis=-1, keepdims=True)
                grouped = off * lax.rsqrt(var + EPS)
                gated[rs, head * DV:(head + 1) * DV] = (g / (1.0 + jnp.exp(-g)) * grouped).astype(BF16)

    def block_of(ref, d, who):
        return ref.at[who, pl.ds(pl.multiple_of(peer(d) * rows, rows), rows), :]

    def reduce_send(part, recv, s_sem, r_sem, who, order):
        for d in range(1, tp):
            copy = pltpu.make_async_remote_copy(
                src_ref=block_of(part, d, who), dst_ref=recv.at[d - 1, who],
                send_sem=s_sem.at[d - 1, order], recv_sem=r_sem.at[d - 1, order],
                device_id=(me_f, peer(d)), device_id_type=MESH)
            copy.start()
            started.append(copy)

    def reduce_wait(recv, s_sem, r_sem, who, order):
        for d in range(1, tp):
            here = recv.at[d - 1, who]
            pltpu.make_async_remote_copy(
                src_ref=here, dst_ref=here, send_sem=s_sem.at[d - 1, order],
                recv_sem=r_sem.at[d - 1, order], device_id=(me_f, peer(d)),
                device_id_type=MESH).wait_recv()

    def total_into(dst_ref, base_ref, part, recv, who):
        width = part.shape[2]
        cols = pl.ds(pl.multiple_of(who * width, width), width)
        total = part[who, my_rows, :].astype(F32)
        for d in range(1, tp):
            total = total + recv[d - 1, who].astype(F32)
        dst_ref[:, cols] = (base_ref[:, cols].astype(F32) + total).astype(BF16)

    def lift():
        width = hidden.shape[1]
        t = tile_of(width)

        @pl.loop(0, width // t)
        def _(j):
            cols = pl.ds(pl.multiple_of(j * t, t), t)
            up = jnp.maximum(jnp.dot(xn2[...], wu[:, cols], preferred_element_type=F32), 0.0)
            hidden[:, cols] = (up * up).astype(BF16)

    def lower(who, order):
        part2[who] = jnp.dot(hidden[...], wd[who], preferred_element_type=F32).astype(BF16)
        reduce_send(part2, recv2, rs2_send, rs2_recv, who, order)

    norm_into(xn, resid_ref, mix_gain_ref)
    ag_start(0, xn)

    def stage(k):
        if k == per - 1:
            own[0].wait()
            ag_wait(0, xn)
            project()
        elif k == per + 1:
            retain()
        elif k == 2 * per - 1:
            own[1].wait()

            @pl.loop(0, fs)
            def _(j):
                part1[j] = jnp.dot(gated[...], wo[j], preferred_element_type=F32).astype(BF16)
            for j in range(fs):
                reduce_send(part1, recv1, rs1_send, rs1_recv, j, j)
        elif k == 3 * per - 3:
            for j in range(fs):
                reduce_wait(recv1, rs1_send, rs1_recv, j, j)

            @pl.loop(0, fs)
            def _(j):
                total_into(after, resid_ref, part1, recv1, j)
            norm_into(xn2, after, mlp_gain_ref)
            ag_start(1, xn2)
        elif k == 3 * per + 2:
            own[2].wait()
            ag_wait(1, xn2)
            lift()
            own[3].wait()
            lower(me_f, 0)
            for dist in range(1, 2):
                for way in range(2):
                    lower(owner(way, dist), 2 * dist - 1 + way)
        elif k > 3 * per + 2:
            _, dist, turn = rounds[k]
            if turn == 1:
                for way in range(2):
                    lower(owner(way, dist), 2 * dist - 1 + way)
            elif dist == half:
                lower(owner(0, half), fs - 1)

    for k in range(4 * per):
        arrive(k)
        for extra in own_at.get(k, ()):
            send(extra)
        stage(k)

    slots = [(me_f, 0)]
    for dist in range(1, half):
        slots += [(owner(way, dist), 2 * dist - 1 + way) for way in range(2)]
    slots.append((owner(0, half), fs - 1))
    for who, order in slots:
        reduce_wait(recv2, rs2_send, rs2_recv, who, order)
        total_into(out_ref, after, part2, recv2, who)
    for copy in started:
        copy.wait_send()


def on_device(fs, tp, resid, mix_gain, w_query, w_key, w_value, w_gate, w_output, decay_rate,
              mlp_gain, w_up, w_down):
    rows, width = resid.shape
    tokens = rows * tp
    w_in = jnp.concatenate([w_query, w_key, w_value, w_gate], axis=1)
    rates = jnp.broadcast_to(decay_rate[:, None], (decay_rate.shape[0], 128))
    rounds = 4 * (fs - 1)
    vmem = pl.BlockSpec(memory_space=pltpu.VMEM)
    hbm = pl.BlockSpec(memory_space=pl.ANY)
    dma = pltpu.SemaphoreType.DMA
    cols = width // fs
    return pl.pallas_call(
        functools.partial(kernel, fs, tp),
        out_shape=jax.ShapeDtypeStruct((rows, width), BF16),
        in_specs=[vmem] * 4 + [hbm] * 4,
        out_specs=vmem,
        scratch_shapes=[
            pltpu.VMEM((width, w_in.shape[1]), BF16),
            pltpu.VMEM((fs, w_output.shape[0], cols), BF16),
            pltpu.VMEM((width, w_up.shape[1]), BF16),
            pltpu.VMEM((fs, w_down.shape[0], cols), BF16),
            pltpu.VMEM((tokens, width), BF16),
            pltpu.VMEM((tokens, width), BF16),
            pltpu.VMEM((tokens, w_in.shape[1]), BF16),
            pltpu.VMEM((tokens, w_output.shape[0]), BF16),
            pltpu.VMEM((tokens, w_up.shape[1]), BF16),
            pltpu.VMEM((fs, tokens, cols), BF16),
            pltpu.VMEM((tp - 1, fs, rows, cols), BF16),
            pltpu.VMEM((fs, tokens, cols), BF16),
            pltpu.VMEM((tp - 1, fs, rows, cols), BF16),
            pltpu.VMEM((rows, width), BF16),
            dma((2, rounds)),
            dma((2, rounds)),
            dma((4,)),
            dma((2, tp - 1)),
            dma((2, tp - 1)),
            dma((tp - 1, fs)),
            dma((tp - 1, fs)),
            dma((tp - 1, fs)),
            dma((tp - 1, fs)),
        ],
        compiler_params=pltpu.CompilerParams(
            collective_id=0, has_side_effects=True, vmem_limit_bytes=67043328),
    )(resid, mix_gain[None, :], mlp_gain[None, :], rates, w_in, w_output, w_up, w_down)


def solution(mesh):
    placed = (
        P(("fs", "tp"), None),
        P(),
        P("fs", "tp"),
        P("fs", "tp"),
        P("fs", "tp"),
        P("fs", "tp"),
        P("tp", "fs"),
        P("tp"),
        P(),
        P("fs", "tp"),
        P("tp", "fs"),
    )
    sizes = dict(mesh.shape)
    return jax.shard_map(
        functools.partial(on_device, sizes["fs"], sizes["tp"]), mesh=mesh, in_specs=placed,
        out_specs=P(("fs", "tp"), None), check_vma=False)
```

time: 700 us -> 273 us (0.39)
  waiting for transfers between devices: 600 us -> 0 us
  Pallas kernels: 0 us -> 266 us
  matrix products: 57.6 us -> 0 us
  between operations: 13.5 us -> 0.01 us
  other arithmetic: 14 us -> 2.03 us
  local copies, waits for them, and re-layouts: 13.5 us -> 3.61 us
    all_gather x9 -> x0, waiting for transfers between devices: 510 us -> none  [the longest x1 125 us: on_device(): down_whole = lax.all_gather(w_down, 'fs', axis=1, tiled=True)]
    pallas_call x0 -> x1, Pallas kernels: none -> 266 us  [on_device(): pl.pallas_call(functools.partial(kernel, fs, tp), out_shape=jax.ShapeDtyp...]
    reduce_scatter x2 -> x0, waiting for transfers between devices: 86.1 us -> none  [the longest x1 44.8 us: on_device(): lax.psum_scatter(jnp.dot(hidden, down_whole, preferred_element_type=jnp.f...]
    dot_general x8 -> x0, matrix products: 57.6 us -> none  [the longest x1 25.4 us: on_device(): jnp.dot(hidden, down_whole, preferred_element_type=jnp.float32)]
  transfers between devices with their start and end apart: 11 -> 0, of which waited for: 11 -> 0; matrix products, arithmetic and copies ran while one was open for 6% -> 0% of each run, Pallas kernels for 0% -> 0%
where the time goes in v1:
time: 273 us; the launch traced here: 272 us
  Pallas kernels  266 us (97%)
  local copies, waits for them, and re-layouts  3.61 us (1%)
    pallas_call x1, Pallas kernels, on_device(): pl.pallas_call(functools.partial(kernel, fs, tp), out_shape=jax.ShapeDtyp...  266 us

profile of v1, /device:TPU:0, one launch (start us, length us, event | category | flops | bytes accessed | tf_op | source)
XLA Modules:
  0.0 271.8 jit_solution(10276059227191794592)
XLA Ops:
  0.0 1.3 broadcast_in_dim.14.rate_ref
  1.3 2.0 pad_maximum_fusion.wq_ref
  3.3 266.1 %shard_map.109 = bf16[256,2048]{1,0:T(8,128)(2,1)} custom-call(bf16[256,2048]{1,0:T(8,128)(2,1)} %resid_ref.1, f32[1,2048]{1,0:T(1,128)} %bitcast.2, f32[1,2048]{1,0:T(1,128)} %bitcast.3, f32[2,128]{1,0:T(2,128)} %broadcast_in_dim.14.rate_ref, bf16[256,1536]{1,0:T(8,128)(2,1)} %pad_maximum_fusion.wq_ref, bf16[512,256]{1,0:T(8,128)(2,1)} %wo_ref.1, ...), custom_call_target="tpu_custom_call" | custom-call | tf_op jit(solution)/shard_map/pallas_call | solution.py:311
  269.5 2.3 copy.13

commit v2 on v1

v2 whole, which is shorter than its diff:
```python
import functools

import jax
import jax.numpy as jnp
from jax import lax
from jax.experimental import pallas as pl
from jax.experimental.pallas import tpu as pltpu
from jax.sharding import PartitionSpec as P

DK = 128
DV = 256
LENGTH = 512
MESH = pl.DeviceIdType.MESH
EPS = 1e-06
F32 = jnp.float32
BF16 = jnp.bfloat16


def tile_of(width):
    return 256 if width % 256 == 0 else 128


def kernel(fs, tp, resid_ref, mix_gain_ref, mlp_gain_ref, rate_ref, wq_ref, wo_ref, wu_ref, wd_ref,
           out_ref, wq, wo, wu, wd, xn, xn2, proj, gated, hidden, part1, core1, chip1, part2, chip2,
           after, ring_send, ring_recv, own_sem, ag_send, ag_recv, line_send, line_recv,
           swap_send, swap_recv, core1_send, core1_recv, chip1_send, chip1_recv, all_send, all_recv,
           core2_send, core2_recv, chip2_send, chip2_recv):
    half = fs // 2
    lines = fs // 2
    chips = tp // 2
    rows = resid_ref.shape[0]
    heads = rate_ref.shape[0]
    tokens = rows * tp
    me_f = lax.axis_index("fs")
    me_t = lax.axis_index("tp")
    pair = me_f % 2
    line = me_f // 2
    other_f = 2 * line + 1 - pair
    chip = me_t // 2
    core = me_t % 2
    other_t = 2 * chip + 1 - core

    def place(i):
        col = i % 2
        at = i // 2
        return at * (1 - col) + (fs - 1 - at) * col

    def index(p):
        col = p // half
        return 2 * (p * (1 - col) + (fs - 1 - p) * col) + col

    my_place = place(me_f)
    target = (index((my_place + 1) % fs), index((my_place + fs - 1) % fs))

    def owner(way, dist):
        if way == 0:
            return index((my_place + fs - dist) % fs)
        return index((my_place + dist) % fs)

    def peer(d):
        return (me_t + d) % tp

    def beside(e):
        return 2 * ((chip + e) % chips) + core

    def step_to(way):
        return me_f + 2 if way == 0 else me_f - 2

    def line_has(way, dist):
        return line >= dist if way == 0 else line + dist <= lines - 1

    def line_next(way):
        return line_has(1 - way, 1)

    barrier = pltpu.get_barrier_semaphore()

    def greet(where):
        pl.semaphore_signal(barrier, inc=1, device_id=where, device_id_type=MESH)

    for way in range(2):
        greet((target[way], me_t))
    for d in range(1, tp):
        greet((me_f, peer(d)))
        if d % 2 == 0:
            greet((other_f, peer(d)))
    greet((other_f, me_t))
    for way in range(2):
        at = (line + (1 if way == 0 else lines - 1)) % lines
        greet((2 * at + pair, me_t))
    pl.semaphore_wait(barrier, 2 + (tp - 1) + (chips - 1) + 1 + 2)

    groups = ((wq_ref, wq, False), (wo_ref, wo, True))
    started = []

    def go(copy, on=None):
        if on is None:
            copy.start()
        else:
            @pl.when(on)
            def _():
                copy.start()
        started.append((copy, on))

    def remote(src, dst, s_sem, r_sem, where):
        return pltpu.make_async_remote_copy(
            src_ref=src, dst_ref=dst, send_sem=s_sem, recv_sem=r_sem, device_id=where,
            device_id_type=MESH)

    def landed(dst, s_sem, r_sem):
        return remote(dst, dst, s_sem, r_sem, (me_f, other_t))

    def span(at, size):
        return pl.ds(pl.multiple_of(at, size), size)

    def slot(w, who, h):
        source, whole, slotted = groups[w]
        deep = source.shape[0]
        hr = deep // 2
        if slotted:
            return whole.at[who, pl.ds(h * hr, hr), :]
        return whole.at[pl.ds(pl.multiple_of(who * deep + h * hr, hr), hr), :]

    rounds = []
    for w in range(2):
        for dist in range(1, half):
            rounds += [(w, dist, 0), (w, dist, 1)]
        rounds.append((w, half, 0))
    per = fs - 1

    def half_of(way, turn):
        return turn if way == 0 else 1 - turn

    def send(k):
        w, dist, turn = rounds[k]
        for way in range(2):
            h = half_of(way, turn)
            who = owner(way, dist - 1)
            source = groups[w][0]
            hr = source.shape[0] // 2
            src = source.at[pl.ds(h * hr, hr), :] if dist == 1 else slot(w, who, h)
            go(remote(src, slot(w, who, h), ring_send.at[way, k], ring_recv.at[way, k],
                      (target[way], me_t)))

    def arrive(k):
        w, dist, turn = rounds[k]
        for way in range(2):
            here = slot(w, owner(way, dist), half_of(way, turn))
            landed(here, ring_send.at[way, k], ring_recv.at[way, k]).wait_recv()
        if dist + 1 < half or (dist + 1 == half and turn == 0):
            send(k + 2)

    up_cols = wu.shape[1]
    deep = wu_ref.shape[0]
    down_rows = wd.shape[1]

    def piece(g, who):
        return wu.at[span(who * deep, deep), :] if g == 0 else wd.at[who]

    def share(g, y):
        if g == 0:
            return wu_ref.at[:, span(y * up_cols, up_cols)]
        return wd_ref.at[span(y * down_rows, down_rows), :]

    def swap_start(g):
        go(remote(share(g, 1 - pair), piece(g, me_f), swap_send.at[g], swap_recv.at[g],
                  (other_f, me_t)))

    def swap_wait(g):
        landed(piece(g, other_f), swap_send.at[g], swap_recv.at[g]).wait_recv()

    line_rounds = [(g, dist, turn) for g in range(2) for dist in range(1, lines) for turn in range(2)]
    per_line = 2 * (lines - 1)

    def line_owner(way, dist, turn):
        at = line - dist if way == 0 else line + dist
        return 2 * at + (pair if turn == 0 else 1 - pair)

    def line_send_round(m, ways=(0, 1)):
        g, dist, turn = line_rounds[m]
        for way in ways:
            who = line_owner(way, dist - 1, turn)
            src = share(g, pair) if dist == 1 and turn == 0 else piece(g, who)
            on = line_next(way) if dist == 1 else jnp.logical_and(line_next(way), line_has(way, dist - 1))
            go(remote(src, piece(g, who), line_send.at[way, m], line_recv.at[way, m],
                      (step_to(way), me_t)), on)

    def line_arrive(m):
        g, dist, turn = line_rounds[m]
        for way in range(2):
            copy = landed(piece(g, line_owner(way, dist, turn)), line_send.at[way, m],
                          line_recv.at[way, m])

            @pl.when(line_has(way, dist))
            def _():
                copy.wait_recv()
            if dist + 1 < lines:
                line_send_round(m + 2, (way,))

    send(0)
    send(1)
    own = []
    for n, (src, dst) in enumerate((
            (wq_ref, wq.at[span(me_f * wq_ref.shape[0], wq_ref.shape[0]), :]),
            (wo_ref, wo.at[me_f]),
            (share(0, pair), piece(0, me_f)),
            (share(1, pair), piece(1, me_f)))):
        copy = pltpu.make_async_copy(src, dst, own_sem.at[n])
        own.append(copy)
    own[0].start()

    my_rows = span(me_t * rows, rows)

    def norm(source, gain_ref):
        wide = source.astype(F32)
        mean = jnp.mean(wide * wide, axis=-1, keepdims=True)
        return (wide * lax.rsqrt(mean + EPS) * gain_ref[...]).astype(BF16)

    step = 64

    def norm_into(buf, first, source_ref, gain_ref):
        @pl.loop(0, rows // step)
        def _(i):
            at = pl.multiple_of(i * step, step)
            buf[pl.ds(pl.multiple_of(first + at, step), step), :] = norm(
                source_ref[pl.ds(at, step), :], gain_ref)

    def ag_block(t):
        return xn.at[span(t * rows, rows), :]

    ag_copies = [remote(ag_block(me_t), ag_block(me_t), ag_send.at[d - 1], ag_recv.at[d - 1],
                        (me_f, peer(d))) for d in range(1, tp)]

    def ag_start():
        for copy in ag_copies:
            copy.start()

    def ag_wait():
        for d in range(1, tp):
            landed(ag_block(peer(tp - d)), ag_send.at[d - 1], ag_recv.at[d - 1]).wait_recv()

    def project():
        width = proj.shape[1]
        t = tile_of(width)

        @pl.loop(0, width // t)
        def _(j):
            cols = pl.ds(pl.multiple_of(j * t, t), t)
            proj[:, cols] = jnp.dot(xn[...], wq[:, cols], preferred_element_type=F32).astype(BF16)

    def retain():
        kq = heads * DK
        vq = heads * DV
        count = tokens // LENGTH
        for head in range(heads):
            rate = rate_ref[head:head + 1, 0:1]

            @pl.loop(0, count)
            def _(n):
                base = pl.multiple_of(n * LENGTH, LENGTH)
                rs = pl.ds(base, LENGTH)
                q = proj[rs, head * DK:(head + 1) * DK]
                k = proj[rs, kq + head * DK:kq + (head + 1) * DK]
                v = proj[rs, 2 * kq + head * DV:2 * kq + (head + 1) * DV]
                g = proj[rs, 2 * kq + vq + head * DV:2 * kq + vq + (head + 1) * DV].astype(F32)
                scores = lax.dot_general(q, k, (((1,), (1,)), ((), ())), preferred_element_type=F32)
                t_at = lax.broadcasted_iota(jnp.int32, (LENGTH, LENGTH), 0)
                s_at = lax.broadcasted_iota(jnp.int32, (LENGTH, LENGTH), 1)
                gap = t_at - s_at
                decay = jnp.exp(-rate * jnp.maximum(gap, 0).astype(F32)) * (DK ** -0.5)
                scores = jnp.where(gap >= 0, scores * decay, 0.0).astype(BF16)
                mixed = jnp.dot(scores, v, preferred_element_type=F32)
                mean = jnp.mean(mixed, axis=-1, keepdims=True)
                off = mixed - mean
                var = jnp.mean(off * off, axis=-1, keepdims=True)
                grouped = off * lax.rsqrt(var + EPS)
                gated[rs, head * DV:(head + 1) * DV] = (g / (1.0 + jnp.exp(-g)) * grouped).astype(BF16)

    def mix_block(x, c):
        return part1.at[span((2 * x + c) * rows, rows), :]

    def mix_out():
        cols = wo.shape[2]

        @pl.loop(0, fs)
        def _(j):
            part1[:, span(j * cols, cols)] = jnp.dot(
                gated[...], wo[j], preferred_element_type=F32).astype(BF16)
        order = [e % chips for e in range(1, chips + 1)]
        for e in order:
            x = (chip + e) % chips
            go(remote(mix_block(x, 1 - core), core1.at[e], core1_send.at[e], core1_recv.at[e],
                      (me_f, other_t)))
        for e in order:
            landed(core1.at[e], core1_send.at[e], core1_recv.at[e]).wait_recv()
            if e:
                first = beside(e) * rows

                @pl.loop(0, rows // step)
                def _(i):
                    at = pl.ds(pl.multiple_of(first + i * step, step), step)
                    more = core1[e, span(i * step, step), :].astype(F32)
                    part1[at, :] = (part1[at, :].astype(F32) + more).astype(BF16)
                go(remote(ag_mix(beside(e)), chip1.at[e - 1], chip1_send.at[e - 1],
                          chip1_recv.at[e - 1], (me_f, beside(e))))

    def ag_mix(t):
        return part1.at[span(t * rows, rows), :]

    def mix_end():
        for e in range(1, chips):
            landed(chip1.at[e - 1], chip1_send.at[e - 1], chip1_recv.at[e - 1]).wait_recv()

        @pl.loop(0, rows // step)
        def _(i):
            at = span(i * step, step)
            total = part1[pl.ds(pl.multiple_of(me_t * rows + i * step, step), step), :].astype(F32)
            total = total + core1[0, at, :].astype(F32)
            for e in range(1, chips):
                total = total + chip1[e - 1, at, :].astype(F32)
            sum_ = (resid_ref[at, :].astype(F32) + total).astype(BF16)
            after[at, :] = sum_
            xn2[pl.ds(pl.multiple_of(block(pair, me_t) * rows + i * step, step), step), :] = norm(
                sum_, mlp_gain_ref)

    def block(y, t):
        return (t % 2) * (2 * chips) + y * chips + t // 2

    def wide(y, t, part=None):
        first = block(y, t) * rows
        hr = rows // 2
        if part is None:
            return xn2.at[span(first, rows), :]
        return xn2.at[pl.ds(pl.multiple_of(first + part * hr, hr), hr), :]

    more_chips = chips - 1
    pieces = 1 + 3 * more_chips

    def all_copy(n, ref, where):
        go(remote(ref, ref, all_send.at[n], all_recv.at[n], where))

    def all_landed(n, ref):
        landed(ref, all_send.at[n], all_recv.at[n]).wait_recv()

    def across(n, ref):
        all_copy(pieces + n, ref, (me_f, other_t))

    def all_first():
        ref = wide(pair, me_t)
        all_copy(0, ref, (other_f, me_t))
        for e in range(1, chips):
            all_copy(e, ref, (me_f, beside(e)))
        all_copy(2 * pieces, ref, (me_f, other_t))

    def all_second():
        ref = wide(1 - pair, me_t)
        all_landed(0, ref)
        for e in range(1, chips):
            all_copy(more_chips + e, wide(1 - pair, me_t, 0), (me_f, beside(e)))
        across(0, ref)
        for e in range(1, chips):
            t = beside(chips - e)
            all_landed(e, wide(pair, t))
            all_copy(2 * more_chips + e, wide(pair, t, 1), (other_f, me_t))
            across(e, wide(pair, t))

    def all_third():
        for part in range(2):
            for e in range(1, chips):
                n = (1 + part) * more_chips + e
                ref = wide(1 - pair, beside(chips - e), part)
                all_landed(n, ref)
                across(n, ref)
        all_landed(2 * pieces, wide(pair, other_t))
        all_landed(pieces, wide(1 - pair, other_t))
        for e in range(1, chips):
            t = 2 * ((chip + chips - e) % chips) + 1 - core
            all_landed(pieces + e, wide(pair, t))
            for part in range(2):
                all_landed(pieces + (1 + part) * more_chips + e, wide(1 - pair, t, part))

    def lift():
        t = tile_of(up_cols)

        @pl.loop(0, 2)
        def _(i):
            at = span(i * tokens, tokens)

            @pl.loop(0, up_cols // t)
            def _(j):
                cols = span(j * t, t)
                up = jnp.maximum(jnp.dot(xn2[at, :], wu[:, cols], preferred_element_type=F32), 0.0)
                hidden[at, cols] = (up * up).astype(BF16)

    cw = wd.shape[2]
    r2 = 2 * chips - 1

    def mlp_copies(who):
        cols = span(who * cw, cw)
        first = core * tokens
        side = remote(part2.at[span((1 - core) * tokens, tokens), cols], xn.at[:, cols],
                      core2_send.at[who], core2_recv.at[who], (me_f, other_t))
        side_in = landed(xn.at[:, cols], core2_send.at[who], core2_recv.at[who])
        outs, ins = [], []
        n = 0
        for dy in range(2):
            for e in range(chips):
                if dy == 0 and e == 0:
                    continue
                y = pair if dy == 0 else 1 - pair
                t = beside(e)
                dst = chip2.at[n, :, cols]
                outs.append(remote(part2.at[span(block(y, t) * rows, rows), cols], dst,
                                   chip2_send.at[n, who], chip2_recv.at[n, who],
                                   (me_f if dy == 0 else other_f, t)))
                ins.append(landed(dst, chip2_send.at[n, who], chip2_recv.at[n, who]))
                n += 1
        return side, side_in, outs, ins

    finals = []

    def lower(who, on=None):
        side, side_in, outs, ins = mlp_copies(who)
        cols = span(who * cw, cw)
        mine = block(pair, me_t) * rows

        def run():
            @pl.loop(0, 2)
            def _(i):
                at = span(((1 - core) * (1 - i) + core * i) * tokens, tokens)
                part2[at, cols] = jnp.dot(
                    hidden[at, :], wd[who], preferred_element_type=F32).astype(BF16)

                @pl.when(i == 0)
                def _():
                    side.start()
            side_in.wait_recv()

            @pl.loop(0, tokens // 128)
            def _(i):
                at = pl.ds(pl.multiple_of(core * tokens + i * 128, 128), 128)
                more = xn[span(i * 128, 128), cols].astype(F32)
                part2[at, cols] = (part2[at, cols].astype(F32) + more).astype(BF16)
            for copy in outs:
                copy.start()

        def end():
            for copy in ins:
                copy.wait_recv()
            total = part2[span(mine, rows), cols].astype(F32)
            for n in range(r2):
                total = total + chip2[n, :, cols].astype(F32)
            out_ref[:, cols] = (after[:, cols].astype(F32) + total).astype(BF16)
            side.wait_send()
            for copy in outs:
                copy.wait_send()

        if on is None:
            run()
        else:
            pl.when(on)(run)
        finals.append((end, on))

    norm_into(xn, me_t * rows, resid_ref, mix_gain_ref)
    ag_start()
    for copy in own[1:]:
        copy.start()

    own_at = {per - 3: [per], per - 2: [per + 1]}

    for k in range(2 * per):
        arrive(k)
        for extra in own_at.get(k, ()):
            send(extra)
        if k == per - 1:
            line_send_round(0)
            own[0].wait()
            ag_wait()
            project()
        elif k == per:
            swap_start(0)
        elif k == per + 1:
            retain()
        elif k == 2 * per - 2:
            swap_wait(0)
            line_send_round(1)
            swap_start(1)
        elif k == 2 * per - 1:
            own[1].wait()
            mix_out()

    last_d = per_line - 2
    for m in range(2 * per_line):
        line_arrive(m)
        if m == last_d - 1:
            line_send_round(per_line)
        elif m == last_d:
            swap_wait(1)
            line_send_round(per_line + 1)
        if m == max(per_line - 4, 0):
            for copy in ag_copies:
                copy.wait_send()
            mix_end()
            all_first()
        elif m == per_line - 1:
            all_second()
        elif m == per_line:
            own[2].wait()
            own[3].wait()
            all_third()
            lift()
            lower(me_f)
            lower(other_f)
        if m >= per_line:
            _, dist, turn = line_rounds[m]
            for way in range(2):
                lower(line_owner(way, dist, turn), line_has(way, dist))

    for end, on in finals:
        if on is None:
            end()
        else:
            pl.when(on)(end)
    for copy, on in started:
        if on is None:
            copy.wait_send()
        else:
            pl.when(on)(copy.wait_send)


def on_device(fs, tp, resid, mix_gain, w_query, w_key, w_value, w_gate, w_output, decay_rate,
              mlp_gain, w_up, w_down):
    rows, width = resid.shape
    tokens = rows * tp
    w_in = jnp.concatenate([w_query, w_key, w_value, w_gate], axis=1)
    rates = jnp.broadcast_to(decay_rate[:, None], (decay_rate.shape[0], 128))
    chips = tp // 2
    wide = 2 * (1 + 3 * (chips - 1)) + 1
    vmem = pl.BlockSpec(memory_space=pltpu.VMEM)
    hbm = pl.BlockSpec(memory_space=pl.ANY)
    dma = pltpu.SemaphoreType.DMA
    cols = width // fs
    return pl.pallas_call(
        functools.partial(kernel, fs, tp),
        out_shape=jax.ShapeDtypeStruct((rows, width), BF16),
        in_specs=[vmem] * 4 + [hbm] * 4,
        out_specs=vmem,
        scratch_shapes=[
            pltpu.VMEM((width, w_in.shape[1]), BF16),
            pltpu.VMEM((fs, w_output.shape[0], cols), BF16),
            pltpu.VMEM((width, w_up.shape[1] // 2), BF16),
            pltpu.VMEM((fs, w_down.shape[0] // 2, cols), BF16),
            pltpu.VMEM((tokens, width), BF16),
            pltpu.VMEM((2 * tokens, width), BF16),
            pltpu.VMEM((tokens, w_in.shape[1]), BF16),
            pltpu.VMEM((tokens, w_output.shape[0]), BF16),
            pltpu.VMEM((2 * tokens, w_up.shape[1] // 2), BF16),
            pltpu.VMEM((tokens, width), BF16),
            pltpu.VMEM((chips, rows, width), BF16),
            pltpu.VMEM((chips - 1, rows, width), BF16),
            pltpu.VMEM((2 * tokens, width), BF16),
            pltpu.VMEM((2 * chips - 1, rows, width), BF16),
            pltpu.VMEM((rows, width), BF16),
            dma((2, 2 * (fs - 1))),
            dma((2, 2 * (fs - 1))),
            dma((4,)),
            dma((tp - 1,)),
            dma((tp - 1,)),
            dma((2, 2 * (fs - 2))),
            dma((2, 2 * (fs - 2))),
            dma((2,)),
            dma((2,)),
            dma((chips,)),
            dma((chips,)),
            dma((chips - 1,)),
            dma((chips - 1,)),
            dma((wide,)),
            dma((wide,)),
            dma((fs,)),
            dma((fs,)),
            dma((2 * chips - 1, fs)),
            dma((2 * chips - 1, fs)),
        ],
        compiler_params=pltpu.CompilerParams(
            collective_id=0, has_side_effects=True, vmem_limit_bytes=67043328),
    )(resid, mix_gain[None, :], mlp_gain[None, :], rates, w_in, w_output, w_up, w_down)


def solution(mesh):
    placed = (
        P(("fs", "tp"), None),
        P(),
        P("fs", "tp"),
        P("fs", "tp"),
        P("fs", "tp"),
        P("fs", "tp"),
        P("tp", "fs"),
        P("tp"),
        P(),
        P("fs", "tp"),
        P("tp", "fs"),
    )
    sizes = dict(mesh.shape)
    return jax.shard_map(
        functools.partial(on_device, sizes["fs"], sizes["tp"]), mesh=mesh, in_specs=placed,
        out_specs=P(("fs", "tp"), None), check_vma=False)
```

time: 273 us -> 248 us (0.908)
  Pallas kernels: 266 us -> 242 us
    pallas_call x1, Pallas kernels: 266 us -> 242 us  [on_device(): pl.pallas_call(functools.partial(kernel, fs, tp), out_shape=jax.ShapeDtyp...]
where the time goes in v2:
time: 248 us; the launch traced here: 247 us
  Pallas kernels  242 us (98%)
  local copies, waits for them, and re-layouts  3.61 us (1%)
    pallas_call x1, Pallas kernels, on_device(): pl.pallas_call(functools.partial(kernel, fs, tp), out_shape=jax.ShapeDtyp...  242 us

profile of v2, /device:TPU:0, one launch (start us, length us, event | category | flops | bytes accessed | tf_op | source)
XLA Modules:
  0.0 247.4 jit_solution(4431701257516277259)
XLA Ops:
  0.0 1.3 broadcast_in_dim.14.rate_ref
  1.3 2.0 pad_maximum_fusion.wq_ref
  3.3 241.7 %shard_map.109 = bf16[256,2048]{1,0:T(8,128)(2,1)} custom-call(bf16[256,2048]{1,0:T(8,128)(2,1)} %resid_ref.1, f32[1,2048]{1,0:T(1,128)} %bitcast.2, f32[1,2048]{1,0:T(1,128)} %bitcast.3, f32[2,128]{1,0:T(2,128)} %broadcast_in_dim.14.rate_ref, bf16[256,1536]{1,0:T(8,128)(2,1)} %pad_maximum_fusion.wq_ref, bf16[512,256]{1,0:T(8,128)(2,1)} %wo_ref.1, ...), custom_call_target="tpu_custom_call" | custom-call | tf_op jit(solution)/shard_map/pallas_call | solution.py:542
  245.1 2.3 copy.13

commit v3 on v2

--- a/solution.py
+++ b/solution.py
@@ -20,13 +20,15 @@
     return 256 if width % 256 == 0 else 128
 
 
-def kernel(fs, tp, resid_ref, mix_gain_ref, mlp_gain_ref, rate_ref, wq_ref, wo_ref, wu_ref, wd_ref,
+def kernel(fs, tp, resid_ref, mix_gain_ref, mlp_gain_ref, rate_ref, w1_ref, w2_ref, w3_ref, w4_ref, wo_ref, wu_ref, wd_ref,
            out_ref, wq, wo, wu, wd, xn, xn2, proj, gated, hidden, part1, core1, chip1, part2, chip2,
-           after, ring_send, ring_recv, own_sem, ag_send, ag_recv, line_send, line_recv,
+           after, ring_send, ring_recv, own_sem, in_sem, ag_send, ag_recv, line_send, line_recv,
            swap_send, swap_recv, core1_send, core1_recv, chip1_send, chip1_recv, all_send, all_recv,
            core2_send, core2_recv, chip2_send, chip2_recv):
     half = fs // 2
     lines = fs // 2
+    in_refs = (w1_ref, w2_ref, w3_ref, w4_ref)
+    deep_q = w1_ref.shape[0]
     chips = tp // 2
     rows = resid_ref.shape[0]
     heads = rate_ref.shape[0]
@@ -72,6 +74,16 @@
     def line_next(way):
         return line_has(1 - way, 1)
 
+    first_row = pl.multiple_of(me_f * deep_q, deep_q)
+    loads = []
+    left = 0
+    for n, ref in enumerate(in_refs):
+        copy = pltpu.make_async_copy(
+            ref, wq.at[pl.ds(first_row, deep_q), left:left + ref.shape[1]], in_sem.at[n])
+        copy.start()
+        loads.append(copy)
+        left += ref.shape[1]
+
     barrier = pltpu.get_barrier_semaphore()
 
     def greet(where):
@@ -89,7 +101,7 @@
         greet((2 * at + pair, me_t))
     pl.semaphore_wait(barrier, 2 + (tp - 1) + (chips - 1) + 1 + 2)
 
-    groups = ((wq_ref, wq, False), (wo_ref, wo, True))
+    groups = ((None, wq, False), (wo_ref, wo, True))
     started = []
 
     def go(copy, on=None):
@@ -114,8 +126,8 @@
 
     def slot(w, who, h):
         source, whole, slotted = groups[w]
-        deep = source.shape[0]
-        hr = deep // 2
+        hr = (deep_q if w == 0 else source.shape[0]) // 2
+        deep = 2 * hr
         if slotted:
             return whole.at[who, pl.ds(h * hr, hr), :]
         return whole.at[pl.ds(pl.multiple_of(who * deep + h * hr, hr), hr), :]
@@ -135,9 +147,10 @@
         for way in range(2):
             h = half_of(way, turn)
             who = owner(way, dist - 1)
-            source = groups[w][0]
-            hr = source.shape[0] // 2
-            src = source.at[pl.ds(h * hr, hr), :] if dist == 1 else slot(w, who, h)
+            src = slot(w, who, h)
+            if dist == 1 and w == 1:
+                hr = wo_ref.shape[0] // 2
+                src = wo_ref.at[pl.ds(h * hr, hr), :]
             go(remote(src, slot(w, who, h), ring_send.at[way, k], ring_recv.at[way, k],
                       (target[way], me_t)))
 
@@ -196,17 +209,17 @@
             if dist + 1 < lines:
                 line_send_round(m + 2, (way,))
 
+    for copy in loads:
+        copy.wait()
     send(0)
     send(1)
-    own = []
+    own = [None]
     for n, (src, dst) in enumerate((
-            (wq_ref, wq.at[span(me_f * wq_ref.shape[0], wq_ref.shape[0]), :]),
             (wo_ref, wo.at[me_f]),
             (share(0, pair), piece(0, me_f)),
             (share(1, pair), piece(1, me_f)))):
         copy = pltpu.make_async_copy(src, dst, own_sem.at[n])
         own.append(copy)
-    own[0].start()
 
     my_rows = span(me_t * rows, rows)
 
@@ -252,7 +265,7 @@
         vq = heads * DV
         count = tokens // LENGTH
         for head in range(heads):
-            rate = rate_ref[head:head + 1, 0:1]
+            rate = rate_ref[head]
 
             @pl.loop(0, count)
             def _(n):
@@ -473,7 +486,6 @@
             send(extra)
         if k == per - 1:
             line_send_round(0)
-            own[0].wait()
             ag_wait()
             project()
         elif k == per:
@@ -496,12 +508,12 @@
         elif m == last_d:
             swap_wait(1)
             line_send_round(per_line + 1)
-        if m == max(per_line - 4, 0):
+        if m == per_line + (-3):
             for copy in ag_copies:
                 copy.wait_send()
             mix_end()
             all_first()
-        elif m == per_line - 1:
+        elif m == per_line + (-1):
             all_second()
         elif m == per_line:
             own[2].wait()
@@ -531,8 +543,7 @@
               mlp_gain, w_up, w_down):
     rows, width = resid.shape
     tokens = rows * tp
-    w_in = jnp.concatenate([w_query, w_key, w_value, w_gate], axis=1)
-    rates = jnp.broadcast_to(decay_rate[:, None], (decay_rate.shape[0], 128))
+    in_width = w_query.shape[1] + w_key.shape[1] + w_value.shape[1] + w_gate.shape[1]
     chips = tp // 2
     wide = 2 * (1 + 3 * (chips - 1)) + 1
     vmem = pl.BlockSpec(memory_space=pltpu.VMEM)
@@ -542,16 +553,16 @@
     return pl.pallas_call(
         functools.partial(kernel, fs, tp),
         out_shape=jax.ShapeDtypeStruct((rows, width), BF16),
-        in_specs=[vmem] * 4 + [hbm] * 4,
+        in_specs=[vmem] * 3 + [pl.BlockSpec(memory_space=pltpu.SMEM)] + [hbm] * 7,
         out_specs=vmem,
         scratch_shapes=[
-            pltpu.VMEM((width, w_in.shape[1]), BF16),
+            pltpu.VMEM((width, in_width), BF16),
             pltpu.VMEM((fs, w_output.shape[0], cols), BF16),
             pltpu.VMEM((width, w_up.shape[1] // 2), BF16),
             pltpu.VMEM((fs, w_down.shape[0] // 2, cols), BF16),
             pltpu.VMEM((tokens, width), BF16),
             pltpu.VMEM((2 * tokens, width), BF16),
-            pltpu.VMEM((tokens, w_in.shape[1]), BF16),
+            pltpu.VMEM((tokens, in_width), BF16),
             pltpu.VMEM((tokens, w_output.shape[0]), BF16),
             pltpu.VMEM((2 * tokens, w_up.shape[1] // 2), BF16),
             pltpu.VMEM((tokens, width), BF16),
@@ -562,6 +573,7 @@
             pltpu.VMEM((rows, width), BF16),
             dma((2, 2 * (fs - 1))),
             dma((2, 2 * (fs - 1))),
+            dma((3,)),
             dma((4,)),
             dma((tp - 1,)),
             dma((tp - 1,)),
@@ -582,7 +594,8 @@
         ],
         compiler_params=pltpu.CompilerParams(
             collective_id=0, has_side_effects=True, vmem_limit_bytes=67043328),
-    )(resid, mix_gain[None, :], mlp_gain[None, :], rates, w_in, w_output, w_up, w_down)
+    )(resid, mix_gain[None, :], mlp_gain[None, :], decay_rate, w_query, w_key, w_value,
+      w_gate, w_output, w_up, w_down)
 
 
 def solution(mesh):

time: 248 us -> 243 us (0.980)
  no operation moved by 1% of the time
where the time goes in v3:
time: 243 us
  Pallas kernels  241 us (99%)
    pallas_call x1, Pallas kernels, on_device(): pl.pallas_call(functools.partial(kernel, fs, tp), out_shape=jax.ShapeDtyp...  241 us

profile of v3, /device:TPU:0, one launch (start us, length us, event | category | flops | bytes accessed | tf_op | source)
XLA Modules:
  0.0 242.9 jit_solution(6895588465565285535)
XLA Ops:
  0.0 240.6 %shard_map.109 = bf16[256,2048]{1,0:T(8,128)(2,1)} custom-call(bf16[256,2048]{1,0:T(8,128)(2,1)} %resid_ref.1, f32[1,2048]{1,0:T(1,128)} %bitcast.2, f32[1,2048]{1,0:T(1,128)} %bitcast.3, f32[2]{0:T(128)} %rate_ref.1, bf16[256,256]{1,0:T(8,128)(2,1)} %w1_ref.1, bf16[256,256]{1,0:T(8,128)(2,1)} %w2_ref.1, bf16[256,512]{1,0:T(8,128)(2,1)} %w3_ref.1, ...), custom_call_target="tpu_custom_call" | custom-call | tf_op jit(solution)/shard_map/pallas_call | solution.py:553
  240.6 2.3 copy.13

commit v4 on v3

--- a/solution.py
+++ b/solution.py
@@ -486,13 +486,12 @@
             send(extra)
         if k == per - 1:
             line_send_round(0)
+            swap_start(0)
             ag_wait()
             project()
-        elif k == per:
-            swap_start(0)
         elif k == per + 1:
             retain()
-        elif k == 2 * per - 2:
+        elif k == 2 * per - 4:
             swap_wait(0)
             line_send_round(1)
             swap_start(1)

time: 243 us -> 254 us (1.045)
  Pallas kernels: 241 us -> 251 us
    pallas_call x1, Pallas kernels: 241 us -> 251 us  [on_device(): pl.pallas_call(functools.partial(kernel, fs, tp), out_shape=jax.ShapeDtyp...]
where the time goes in v4:
time: 254 us; the launch traced here: 253 us
  Pallas kernels  251 us (99%)
    pallas_call x1, Pallas kernels, on_device(): pl.pallas_call(functools.partial(kernel, fs, tp), out_shape=jax.ShapeDtyp...  251 us

profile of v4, /device:TPU:0, one launch (start us, length us, event | category | flops | bytes accessed | tf_op | source)
XLA Modules:
  0.0 253.5 jit_solution(17550484106037368526)
XLA Ops:
  0.0 251.2 %shard_map.109 = bf16[256,2048]{1,0:T(8,128)(2,1)} custom-call(bf16[256,2048]{1,0:T(8,128)(2,1)} %resid_ref.1, f32[1,2048]{1,0:T(1,128)} %bitcast.2, f32[1,2048]{1,0:T(1,128)} %bitcast.3, f32[2]{0:T(128)} %rate_ref.1, bf16[256,256]{1,0:T(8,128)(2,1)} %w1_ref.1, bf16[256,256]{1,0:T(8,128)(2,1)} %w2_ref.1, bf16[256,512]{1,0:T(8,128)(2,1)} %w3_ref.1, ...), custom_call_target="tpu_custom_call" | custom-call | tf_op jit(solution)/shard_map/pallas_call | solution.py:552
  251.2 2.3 copy.13
